TPU v7x, 512 devices: a whole 4x4x16 slice. The times are simulated.
512 devices in a mesh: ep: 32 (over z, core), tp: 16 (over y, x).
Axes of the slice: x: 4, y: 4, z: 16, core: 2. Of those that a mesh axis runs over, the one named last changes fastest.
Arguments:
- queries: bfloat16 [8192, 2048], P('ep', 'tp'), may hold values from -6 to 6
- keys: bfloat16 [8192, 2048], P('ep', 'tp'), may hold values from -6 to 6
- values: bfloat16 [8192, 2048], P('ep', 'tp'), may hold values from -6 to 6
- gates: bfloat16 [8192, 2048], P('ep', 'tp'), may hold values from -6 to 6
- log_decay: float32 [8192, 16], P('ep', 'tp'), may hold values from -2 to 0
- out_weight: bfloat16 [2048, 2048], P(None, 'tp'), may hold values from -0.125 to 0.125
- moe_rows: bfloat16 [8192, 2048], P('ep'), may hold values from -140 to 140
- moe_gain: bfloat16 [2048], replicated, may hold values from 0.099609375 to 1.8984375
- routes: int32 [8192, 2], P('ep'), may hold values from 0 to 31, as said below
- route_weights: float32 [8192, 2], P('ep'), may hold values from 0.1 to 1
- gate_proj: bfloat16 [32, 2048, 4096], P('ep', None, 'tp'), may hold values from -0.125 to 0.125
- up_proj: bfloat16 [32, 2048, 4096], P('ep', None, 'tp'), may hold values from -0.125 to 0.125
- down_proj: bfloat16 [32, 4096, 2048], P('ep', None, 'tp'), may hold values from -0.09375 to 0.09375
Outputs:
- mixer_out: bfloat16 [8192, 2048], P('ep', 'tp')
- moe_out: bfloat16 [8192, 2048], P('ep', 'tp')
Inputs may be any that keep to these rules, and one draw needn't show every extreme that they name: `routes`: each row names two different experts of one group of 8 consecutive experts; in each aligned block of 256 rows every expert is named by exactly 16 rows.
All inputs are finite; a program needn't handle non-finite values.
Results may differ from a plain program's by a relative error of at most 0.011.
Values may be sent and summed in bfloat16 or wider, within the bound.
No kernel may reach another device: no remote copies, remote signals or barrier semaphores. Data moves between devices by JAX's collectives and lax.ppermute only.
A program may use at most 64 MiB of HBM per device.

v0:
```python
import jax
import jax.numpy as jnp
from jax import lax
from jax.sharding import Mesh
from jax.sharding import PartitionSpec as P

BLOCK = 128
EP = ("ep_0", "ep_1")
TP = ("tp_0", "tp_1")


def filled_with(array, identity):
    return jax.tree.map(
        lambda part, zero: jnp.zeros_like(part) + jnp.asarray(zero, part.dtype), array, identity
    )


def collected_together(array, axis):
    leaves = jax.tree.leaves(array)
    turns = sorted(range(len(leaves)), key=lambda k: -leaves[k].size)
    width = (1, *leaves[turns[0]].shape)[-1]
    lines = [
        jnp.pad(leaves[k].reshape(-1), (0, -leaves[k].size % width)).reshape(-1, width)
        for k in turns
    ]
    both, at, found = (lax.all_gather(jnp.concatenate(lines), axis), 0, {})
    for k, line in zip(turns, lines):
        piece = both[:, at : at + len(line)].reshape(len(both), -1)
        found[k] = piece[:, : leaves[k].size].reshape(-1, *leaves[k].shape)
        at += len(line)
    numbers = iter(range(len(leaves)))
    return jax.tree.map(lambda _: found[next(numbers)], array)


def carried_in(array, axes, combine, identity):
    before = start = filled_with(array, identity)
    total = array
    for axis in reversed(axes):
        peers, mine = (lax.axis_size(axis), lax.axis_index(axis))
        pieces = collected_together(total, axis)
        inside, total = (start, start)
        for k in range(peers):
            passed = k < mine
            total = combine(total, jax.tree.map(lambda part: part[k], pieces))
            inside = jax.tree.map(lambda new, old: jnp.where(passed, new, old), total, inside)
        before = combine(inside, before)
    return before


def whole_of(array, axes, dim):
    for axis in reversed(axes):
        array = lax.all_gather(array, axis, axis=dim, tiled=True)
    return array


def in_order(parts, dim):
    lengths = list(parts.shape[1:])
    lengths[dim] *= parts.shape[0]
    return jnp.moveaxis(parts, 0, dim).reshape(lengths)


def copy_for_each(array, axis):
    peers = lax.axis_size(axis)
    return lax.all_to_all(
        jnp.broadcast_to(array[None], (peers, *array.shape)), axis, 0, 0, tiled=True
    )


def collect(array, axis, dim):
    return in_order(copy_for_each(array, axis), dim)


def rotate(source, positions, heads_here, factor):
    row_count, feat_width = source.shape
    head_dim = feat_width // heads_here
    half_dim = head_dim // 2
    values_f = source.astype(jnp.float32).reshape(row_count, heads_here, head_dim)
    inverse = 10000.0 ** (-jnp.arange(half_dim, dtype=jnp.float32) / half_dim)
    angles = positions[:, None] * inverse[None, :]
    cosine = jnp.cos(angles)[:, None, :]
    sine_part = jnp.sin(angles)[:, None, :]
    first_half = values_f[..., :half_dim]
    second_half = values_f[..., half_dim:]
    turned = jnp.concatenate(
        [
            first_half * cosine - second_half * sine_part,
            first_half * sine_part + second_half * cosine,
        ],
        axis=-1,
    )
    return (turned * factor).astype(jnp.bfloat16).reshape(row_count, feat_width)


def chain_states(earlier, later):
    return (earlier[0] * later[0], later[0][:, None, None] * earlier[1] + later[1])


def retention_half(queries, keys, values, gates, log_decay, out_weight):
    row_count, feat_width = queries.shape
    heads_here = log_decay.shape[1]
    head_dim = feat_width // heads_here
    block_count = row_count // BLOCK
    positions = (lax.axis_index(EP) * row_count + jnp.arange(row_count, dtype=jnp.int32)).astype(
        jnp.float32
    )
    rot_q = rotate(queries, positions, heads_here, 1.0)
    rot_k = rotate(keys, positions, heads_here, head_dim ** (-0.5))
    block_shape = (block_count, BLOCK, heads_here, head_dim)
    q_blocks = rot_q.reshape(block_shape)
    k_blocks = rot_k.reshape(block_shape)
    v_blocks = values.reshape(block_shape)
    cumulative = jnp.cumsum(log_decay.reshape(block_count, BLOCK, heads_here), axis=1)
    across = jnp.swapaxes(cumulative, 1, 2)
    spread = across[..., :, None] - across[..., None, :]
    causal = jnp.arange(BLOCK)[:, None] >= jnp.arange(BLOCK)[None, :]
    weights = jnp.where(causal, jnp.exp(jnp.where(causal, spread, 0.0)), 0.0)
    scores = jnp.einsum("nihd,njhd->nhij", q_blocks, k_blocks, preferred_element_type=jnp.float32)
    rounded = (scores * weights).astype(jnp.bfloat16)
    inside = jnp.einsum("nhij,njhd->nihd", rounded, v_blocks, preferred_element_type=jnp.float32)
    ending = cumulative[:, -1, :]
    k_scaled = k_blocks.astype(jnp.float32) * jnp.exp(ending[:, None, :] - cumulative)[..., None]
    updates = jnp.einsum(
        "njhd,njhe->nhde", k_scaled, v_blocks.astype(jnp.float32), precision=lax.Precision.HIGHEST
    )

    def advance(carry_state, member):
        return (jnp.exp(member[0])[:, None, None] * carry_state + member[1], carry_state)

    zero_state = jnp.zeros((heads_here, head_dim, head_dim), jnp.float32)
    local_end, before = lax.scan(advance, zero_state, (ending, updates))
    device_decay = jnp.exp(jnp.sum(ending, axis=0))
    incoming = carried_in(
        (device_decay, local_end), EP, chain_states, (jnp.ones_like(device_decay), zero_state)
    )
    leading = jnp.cumsum(ending, axis=0) - ending
    entering = before + jnp.exp(leading)[:, :, None, None] * incoming[1][None]
    carried = (
        jnp.einsum(
            "nihd,nhde->nihe",
            q_blocks.astype(jnp.float32),
            entering,
            precision=lax.Precision.HIGHEST,
        )
        * jnp.exp(cumulative)[..., None]
    )
    retained = (inside + carried).reshape(row_count, heads_here, head_dim)
    gate_f = gates.astype(jnp.float32).reshape(row_count, heads_here, head_dim)
    scaled = retained * lax.rsqrt(jnp.mean(retained * retained, axis=-1, keepdims=True) + 1e-05)
    head_out = (scaled * jax.nn.silu(gate_f)).astype(jnp.bfloat16).reshape(row_count, feat_width)
    projected = jnp.dot(whole_of(head_out, TP, 1), out_weight, preferred_element_type=jnp.float32)
    return projected.astype(jnp.bfloat16)


def expert_half(moe_rows, moe_gain, routes, route_weights, gate_proj, up_proj, down_proj):
    row_count, feat_width = moe_rows.shape
    experts = lax.axis_size(EP)
    capacity = 2 * row_count // experts
    as_float = moe_rows.astype(jnp.float32)
    normed = (
        as_float
        * lax.rsqrt(jnp.mean(as_float * as_float, axis=-1, keepdims=True) + 1e-06)
        * moe_gain.astype(jnp.float32)
    ).astype(jnp.bfloat16)
    flat_ids = routes.reshape(-1)
    onehot = (flat_ids[:, None] == jnp.arange(experts, dtype=jnp.int32)[None, :]).astype(jnp.int32)
    slot_rank = jnp.sum((jnp.cumsum(onehot, axis=0) - onehot) * onehot, axis=1)
    target = flat_ids * capacity + slot_rank
    source_row = (
        jnp.zeros((experts * capacity,), jnp.int32)
        .at[target]
        .set(jnp.arange(2 * row_count, dtype=jnp.int32) // 2)
    )
    outgoing = normed[source_row].reshape(experts, capacity, feat_width)
    w_gate = gate_proj[0]
    w_up = up_proj[0]
    w_down = down_proj[0]
    share_size = capacity // lax.axis_size(TP)
    own_share = lax.dynamic_slice_in_dim(outgoing, lax.axis_index(TP) * share_size, share_size, 1)
    arrived_share = lax.all_to_all(own_share, EP, split_axis=0, concat_axis=0, tiled=True)
    arrived = collect(arrived_share, TP, 1)
    gate_part = jnp.einsum("scd,df->scf", arrived, w_gate, preferred_element_type=jnp.float32)
    up_part = jnp.einsum("scd,df->scf", arrived, w_up, preferred_element_type=jnp.float32)
    hidden = (jax.nn.silu(gate_part) * up_part).astype(jnp.bfloat16)
    expert_out = jnp.einsum(
        "scf,fd->scd",
        lax.all_gather(hidden, TP, axis=2, tiled=True),
        w_down,
        preferred_element_type=jnp.float32,
    ).astype(jnp.bfloat16)
    returned = lax.all_to_all(expert_out, EP, split_axis=0, concat_axis=0, tiled=True)
    picked = returned.reshape(experts * capacity, -1)[target].reshape(row_count, 2, -1)
    return jnp.sum(picked.astype(jnp.float32) * route_weights[:, :, None], axis=1).astype(
        jnp.bfloat16
    )


def on_device(
    queries,
    keys,
    values,
    gates,
    log_decay,
    out_weight,
    moe_rows,
    moe_gain,
    routes,
    route_weights,
    gate_proj,
    up_proj,
    down_proj,
):
    mixer_out = retention_half(queries, keys, values, gates, log_decay, out_weight)
    moe_out = expert_half(moe_rows, moe_gain, routes, route_weights, gate_proj, up_proj, down_proj)
    return (mixer_out, moe_out)


def solution(mesh):
    torus = Mesh(mesh.devices.reshape(16, 2, 4, 4), ("ep_0", "ep_1", "tp_0", "tp_1"))
    return jax.shard_map(
        on_device,
        mesh=torus,
        in_specs=(
            P(EP, TP),
            P(EP, TP),
            P(EP, TP),
            P(EP, TP),
            P(EP, TP),
            P(None, TP),
            P(EP, None),
            P(),
            P(EP, None),
            P(EP, None),
            P(EP, None, TP),
            P(EP, None, TP),
            P(EP, None, TP),
        ),
        out_specs=(P(EP, TP), P(EP, TP)),
        check_vma=False,
    )
```

profile of v0, /device:TPU:2, one launch (start us, length us, event | category | flops | bytes accessed | tf_op | source)
XLA Modules:
  0.0 250.1 jit_solution(12538296000440214369)
XLA Ops:
  7.2 1.0 copy.44
  8.2 0.1 eq.29
  8.3 0.1 eq.25
  8.4 0.7 broadcast_multiply_fusion
  9.1 1.2 reduce-window.18
  10.3 0.2 slice_reduce_fusion
  10.6 0.1 copy.43
  10.7 0.1 mul.536
  10.9 0.1 fusion.53
  11.0 2.4 scatter_custom_fusion
  13.5 0.7 convert_element_type.89
  14.2 1.5 fusion
  15.7 0.3 fusion.2
  16.0 3.3 %gather_fusion = bf16[512,2048]{1,0:T(8,128)(2,1)} fusion(bf16[256,2048]{1,0:T(8,128)(2,1)S(1)} %fusion.2, s32[1024]{0:T(1024)S(1)} %pad_clamp_fusion.1), kind=kCustom, calls=%fused_computation | custom fusion | bytes 4196352 | tf_op jit(solution)/shard_map/gather | solution.py:173
  19.4 1.5 constant_dynamic-slice_fusion.1
  20.9 0.5 broadcast.370
  21.4 1.4 reduce.10
  22.8 0.7 reshape.656
  23.5 15.5 %all-to-all-start = ((bf16[32,2,1024]{2,1,0:T(2,128)(2,1)}), bf16[32,2,1024]{2,1,0:T(2,128)(2,1)S(1)}, u32[]{:S(2)}, u32[]{:S(2)}) async-start(bf16[32,2,1024]{2,1,0:T(2,128)(2,1)} %reshape.656), calls=%async_computation | async-start | bytes 262144 | tf_op jit(solution)/shard_map/all_to_all | solution.py:179
  39.1 0.1 copy.40
  39.2 0.2 reduce_window_sum.33
  39.4 0.6 slice_reduce_fusion.1
  40.0 0.1 reduce.4
  40.2 0.6 fusion.34
  40.8 0.1 fusion.39
  40.9 0.6 fusion.80
  41.5 0.4 convolution_bitcast_fusion.1
  41.9 2.4 while.13
  41.9 0.6 fusion.88
  42.5 0.6 bitcast_add_fusion.2
  43.1 0.6 fusion.88
  43.7 0.6 bitcast_add_fusion.2
  44.9 0.5 pad_bitcast_fusion.1
  45.5 10.7 %all-to-all-done = bf16[32,2,1024]{2,1,0:T(2,128)(2,1)S(1)} async-done(((bf16[32,2,1024]{2,1,0:T(2,128)(2,1)}), bf16[32,2,1024]{2,1,0:T(2,128)(2,1)S(1)}, u32[]{:S(2)}, u32[]{:S(2)}) %all-to-all-start) | async-done | bytes 131104 | tf_op jit(solution)/shard_map/all_to_all | solution.py:179
  56.2 0.1 reshape.657
  56.4 1.6 broadcast_in_dim.33
  58.0 7.5 %all-to-all-start.1 = ((bf16[16,32,1,2048]{3,1,2,0:T(8,128)(2,1)}), bf16[16,32,1,2048]{3,1,2,0:T(8,128)(2,1)S(1)}, u32[]{:S(2)}, u32[]{:S(2)}) async-start(bf16[16,32,1,2048]{3,1,2,0:T(8,128)(2,1)} %broadcast_in_dim.33), calls=%async_computation.1 | async-start | bytes 4194304 | tf_op jit(solution)/shard_map/all_to_all | solution.py:64
  65.6 1.9 all-gather.2
  67.5 0.6 fusion.79
  70.0 0.7 fusion.66
  70.6 0.6 maximum_bitcast_fusion.1
  71.3 20.4 %all-to-all-done.1 = bf16[16,32,1,2048]{3,1,2,0:T(8,128)(2,1)S(1)} async-done(((bf16[16,32,1,2048]{3,1,2,0:T(8,128)(2,1)}), bf16[16,32,1,2048]{3,1,2,0:T(8,128)(2,1)S(1)}, u32[]{:S(2)}, u32[]{:S(2)}) %all-to-all-start.1) | async-done | bytes 2097184 | tf_op jit(solution)/shard_map/all_to_all | solution.py:64
  91.7 0.7 fusion.5
  92.5 0.5 copy-done.12
  92.9 1.4 fusion.10
  94.5 0.9 reduce-window.14
  96.0 0.6 fusion.72
  96.6 36.7 %all-gather.12.cloned.1.call-done = f32[16,129,128]{2,1,0:T(8,128)} async-done(((f32[1,129,128]{2,1,0:T(8,128)}), f32[16,129,128]{2,1,0:T(8,128)}) %all-gather.12.cloned.1.call-update) | async-done | bytes 1056784 | tf_op jit(solution)/shard_map/all_gather | solution.py:26
  133.3 0.8 slice.250
  134.2 0.6 fusion.78
  135.4 11.5 %fusion.57 = f32[128,128]{1,0:T(8,128)S(1)} fusion(f32[16,129,128]{2,1,0:T(8,128)} %all-gather.12.cloned.1.call-done, f32[2,129,128]{2,1,0:T(8,128)S(1)} %all-gather.2, f32[]{:T(128)} %bitcast.46, f32[]{:T(128)} %bitcast.45, f32[]{:T(128)} %bitcast.44, f32[]{:T(128)} %bitcast.43, f32[]{:T(128)} %bitcast.42, f32[]{:T(128)} %bitcast.41, f32[]{:T(128)} %bitcast.40, ...), kind=kLoop, calls=%fused_computation.81 | loop fusion | flops 884736 | bytes 1245278 | tf_op jit(solution)/shard_map/mul | solution.py:136
  146.9 1.2 fusion.14
  148.1 0.4 fusion.40
  148.6 0.1 fusion.50
  148.7 13.4 %all_gather.25 = bf16[256,512]{1,0:T(8,128)(2,1)} all-gather(bf16[256,128]{1,0:T(8,128)(2,1)S(1)} %fusion.50), channel_id=1, replica_groups=mesh['ep_0'=16,'ep_1'=2,'tp_0'=4,'tp_1'=4] {'tp_1'}, dimensions={1}, use_global_device_ids=true | all-gather | bytes 327680 | tf_op jit(solution)/shard_map/all_gather | solution.py:52
  162.2 43.0 %all-gather.10.cloned.1.call-done = bf16[32,16,4096]{2,0,1:T(8,128)(2,1)} async-done(((bf16[32,16,256]{2,0,1:T(8,128)(2,1)}), bf16[32,16,4096]{2,0,1:T(8,128)(2,1)}) %all-gather.10.cloned.1.call-update) | async-done | bytes 4194320 | tf_op jit(solution)/shard_map/all_gather | solution.py:186
  205.2 3.4 %fusion.16 = bf16[32,16,128]{2,0,1:T(8,128)(2,1)S(1)} fusion(bf16[32,16,4096]{2,0,1:T(8,128)(2,1)} %all-gather.10.cloned.1.call-done, bf16[1,4096,128]{2,1,0:T(8,128)(2,1)S(1)} %copy-done.13), kind=kOutput, calls=%fused_computation.25 | convolution fusion | flops 536870912 | bytes 5373952 | tf_op jit(solution)/shard_map/scf,fd->scd/dot_general | solution.py:184
  208.6 0.7 copy.58
  209.3 12.6 %all-to-all-start.2 = ((bf16[32,16,128]{2,1,0:T(8,128)(2,1)}), bf16[32,16,128]{2,1,0:T(8,128)(2,1)S(1)}, u32[]{:S(2)}, u32[]{:S(2)}) async-start(bf16[32,16,128]{2,1,0:T(8,128)(2,1)} %copy.58), calls=%async_computation.2 | async-start | bytes 262144 | tf_op jit(solution)/shard_map/all_to_all | solution.py:190
  221.9 0.1 copy.49
  222.1 16.8 %all-gather.8.cloned.1.call-done = bf16[256,2048]{1,0:T(8,128)(2,1)} async-done(((bf16[256,512]{1,0:T(8,128)(2,1)}), bf16[256,2048]{1,0:T(8,128)(2,1)}) %all-gather.8.cloned.1.call-update) | async-done | bytes 1048592 | tf_op jit(solution)/shard_map/all_gather | solution.py:52
  238.9 2.3 convolution_convert_fusion
  241.2 1.3 gather_fusion.1
  242.5 1.1 fusion.20
  (56 shorter events, 0.5 us)
Async XLA Ops:
  7.2 84.6 %copy-start = (bf16[1,2048,256]{2,1,0:T(8,128)(2,1)S(1)}, bf16[1,2048,256]{2,1,0:T(8,128)(2,1)}, u32[]{:S(2)}) copy-start(bf16[1,2048,256]{2,1,0:T(8,128)(2,1)} %param.25) | copy-start | bytes 3145732
  7.2 8.5 %copy-start.1 = (bf16[256,2048]{1,0:T(8,128)(2,1)S(1)}, bf16[256,2048]{1,0:T(8,128)(2,1)}, u32[]{:S(2)}) copy-start(bf16[256,2048]{1,0:T(8,128)(2,1)} %param.21) | copy-start | bytes 3145732
  16.0 23.1 %copy-start.10 = (f32[256,1]{0,1:T(1,128)S(1)}, f32[256,1]{0,1:T(1,128)}, u32[]{:S(2)}) copy-start(f32[256,1]{0,1:T(1,128)} %param.19) | copy-start | bytes 3076
  16.0 24.1 %copy-start.4 = (bf16[256,128]{1,0:T(8,128)(2,1)S(1)}, bf16[256,128]{1,0:T(8,128)(2,1)}, u32[]{:S(2)}) copy-start(bf16[256,128]{1,0:T(8,128)(2,1)} %param.16) | copy-start | bytes 196612
  16.0 24.1 %copy-start.5 = (bf16[256,128]{1,0:T(8,128)(2,1)S(1)}, bf16[256,128]{1,0:T(8,128)(2,1)}, u32[]{:S(2)}) copy-start(bf16[256,128]{1,0:T(8,128)(2,1)} %param.15) | copy-start | bytes 196612
  19.4 22.1 %copy-start.6 = (bf16[256,128]{1,0:T(8,128)(2,1)S(1)}, bf16[256,128]{1,0:T(8,128)(2,1)}, u32[]{:S(2)}) copy-start(bf16[256,128]{1,0:T(8,128)(2,1)} %param.17) | copy-start | bytes 196612
  23.5 32.7 %all-to-all-start = ((bf16[32,2,1024]{2,1,0:T(2,128)(2,1)}), bf16[32,2,1024]{2,1,0:T(2,128)(2,1)S(1)}, u32[]{:S(2)}, u32[]{:S(2)}) async-start(bf16[32,2,1024]{2,1,0:T(2,128)(2,1)} %reshape.656), calls=%async_computation | async-start | bytes 262144 | tf_op jit(solution)/shard_map/all_to_all | solution.py:179
  44.3 1.2 copy-start.3
  44.3 13.7 %copy-start.9 = (f32[2,1]{0,1:T(1,128)}, f32[2,1]{0,1:T(1,128)S(1)}, u32[]{:S(2)}) copy-start(f32[2,1]{0,1:T(1,128)S(1)} %get-tuple-element.178) | copy-start | bytes 28
  58.0 7.5 %copy-start.11 = (f32[1,128]{1,0:T(1,128)S(1)}, f32[1,128]{1,0:T(1,128)}, u32[]{:S(2)}) copy-start(f32[1,128]{1,0:T(1,128)} %pad_bitcast_fusion.1) | copy-start | bytes 1540
  58.0 33.7 %all-to-all-start.1 = ((bf16[16,32,1,2048]{3,1,2,0:T(8,128)(2,1)}), bf16[16,32,1,2048]{3,1,2,0:T(8,128)(2,1)S(1)}, u32[]{:S(2)}, u32[]{:S(2)}) async-start(bf16[16,32,1,2048]{3,1,2,0:T(8,128)(2,1)} %broadcast_in_dim.33), calls=%async_computation.1 | async-start | bytes 4194304 | tf_op jit(solution)/shard_map/all_to_all | solution.py:64
  65.5 67.8 %all-gather.12.cloned.1.call-start = ((), (), s32[]{:S(2)}) async-start(), calls=%async_computation.5 | async-start | bytes 1183744 | tf_op jit(solution)/shard_map/all_gather | solution.py:26
  71.3 133.9 %all-gather.10.cloned.1.call-start = ((), (), s32[]{:S(2)}) async-start(), calls=%async_computation.4 | async-start | bytes 4456448 | tf_op jit(solution)/shard_map/all_gather | solution.py:186
  91.7 1.2 copy-start.12
  94.4 54.2 %copy-start.7 = (bf16[256,128]{1,0:T(8,128)(2,1)S(1)}, bf16[256,128]{1,0:T(8,128)(2,1)}, u32[]{:S(2)}) copy-start(bf16[256,128]{1,0:T(8,128)(2,1)} %param.18) | copy-start | bytes 196612
  94.4 110.8 %copy-start.13 = (bf16[1,4096,128]{2,1,0:T(8,128)(2,1)S(1)}, bf16[1,4096,128]{2,1,0:T(8,128)(2,1)}, u32[]{:S(2)}) copy-start(bf16[1,4096,128]{2,1,0:T(8,128)(2,1)} %param.27) | copy-start | bytes 3145732
  94.4 144.5 %all-gather.8.cloned.1.call-start = ((), (), s32[]{:S(2)}) async-start(), calls=%async_computation.3 | async-start | bytes 1310720 | tf_op jit(solution)/shard_map/all_gather | solution.py:52
  162.1 59.7 %copy-start.8 = (f32[256,2]{0,1:T(2,128)S(1)}, f32[256,2]{0,1:T(2,128)}, u32[]{:S(2)}) copy-start(f32[256,2]{0,1:T(2,128)} %param.24) | copy-start | bytes 6148
  162.2 76.7 %copy-start.2 = (bf16[2048,128]{1,0:T(8,128)(2,1)S(1)}, bf16[2048,128]{1,0:T(8,128)(2,1)}, u32[]{:S(2)}) copy-start(bf16[2048,128]{1,0:T(8,128)(2,1)} %param.20) | copy-start | bytes 1572868
  209.3 31.9 %all-to-all-start.2 = ((bf16[32,16,128]{2,1,0:T(8,128)(2,1)}), bf16[32,16,128]{2,1,0:T(8,128)(2,1)S(1)}, u32[]{:S(2)}, u32[]{:S(2)}) async-start(bf16[32,16,128]{2,1,0:T(8,128)(2,1)} %copy.58), calls=%async_computation.2 | async-start | bytes 262144 | tf_op jit(solution)/shard_map/all_to_all | solution.py:190
Sparse Core Ops, SparseCore 0:
  71.4 61.8 all-gather.11
  136.3 68.8 all-gather.9
  207.3 31.5 all-gather.7
where the time goes:
time: 251 us; the launch traced here: 250 us
  waiting for transfers between devices  128 us (51%)
  starting transfers between devices  35.6 us (14%)
  other arithmetic  24.8 us (10%)
  local copies, waits for them, and re-layouts  18.7 us (7%)
  between operations  18 us (7%)
  blocking collectives  15.3 us (6%)
  matrix products  9.84 us (4%)
    all_gather x1, waiting for transfers between devices, expert_half(): lax.all_gather(hidden, TP, axis=2, tiled=True)  43 us
    all_gather x1, waiting for transfers between devices, collected_together(): both, at, found = (lax.all_gather(jnp.concatenate(lines), axis), 0, {})  36.7 us
    all_to_all x1, waiting for transfers between devices, copy_for_each(): lax.all_to_all(jnp.broadcast_to(array[None], (peers, *array.shape)), axis...  20.4 us
    all_gather x1, waiting for transfers between devices, whole_of(): array = lax.all_gather(array, axis, axis=dim, tiled=True)  16.8 us
    all_to_all x1, starting transfers between devices, expert_half(): lax.all_to_all(own_share, EP, split_axis=0, concat_axis=0, tiled=True)  15.5 us
    all_gather x1, blocking collectives, whole_of(): array = lax.all_gather(array, axis, axis=dim, tiled=True)  13.4 us
    all_to_all x1, starting transfers between devices, expert_half(): lax.all_to_all(expert_out, EP, split_axis=0, concat_axis=0, tiled=True)  12.6 us
    mul x1, other arithmetic, retention_half(): entering = before + jnp.exp(leading)[:, :, None, None] * incoming[1][None]  11.5 us
  transfers between devices with their start and end apart: 6, of which 5 were waited for; matrix products, arithmetic and copies ran while one was open for 13% of the time, Pallas kernels for 0%

commit v1 on v0

--- a/solution.py
+++ b/solution.py
@@ -7,6 +7,16 @@
 BLOCK = 128
 EP = ("ep_0", "ep_1")
 TP = ("tp_0", "tp_1")
+
+
+def tiles_fit(original, along_dim, along_axis):
+    xs_all = []
+    for _ in range(jax.lax.axis_size(along_axis)):
+        xs_all.append(original)
+    known = jnp.stack(xs_all, axis=0)
+    e_next = jax.lax.all_to_all(known, along_axis, 0, 0)
+    newest = jnp.concatenate(e_next, axis=along_dim)
+    return newest
 
 
 def filled_with(array, identity):
@@ -182,10 +192,7 @@
     up_part = jnp.einsum("scd,df->scf", arrived, w_up, preferred_element_type=jnp.float32)
     hidden = (jax.nn.silu(gate_part) * up_part).astype(jnp.bfloat16)
     expert_out = jnp.einsum(
-        "scf,fd->scd",
-        lax.all_gather(hidden, TP, axis=2, tiled=True),
-        w_down,
-        preferred_element_type=jnp.float32,
+        "scf,fd->scd", tiles_fit(hidden, 2, TP), w_down, preferred_element_type=jnp.float32
     ).astype(jnp.bfloat16)
     returned = lax.all_to_all(expert_out, EP, split_axis=0, concat_axis=0, tiled=True)
     picked = returned.reshape(experts * capacity, -1)[target].reshape(row_count, 2, -1)

time: 251 us -> 213 us (0.85)
  waiting for transfers between devices: 128 us -> 76.7 us
  local copies, waits for them, and re-layouts: 18.7 us -> 24.8 us
  starting transfers between devices: 35.6 us -> 41.4 us
  blocking collectives: 15.3 us -> 19.3 us
  matrix products: 9.84 us -> 6.72 us
    all_gather x1 -> x0, waiting for transfers between devices: 43 us -> none  [expert_half(): lax.all_gather(hidden, TP, axis=2, tiled=True)]
    all_to_all x0 -> x1, starting transfers between devices: none -> 8.12 us  [tiles_fit(): e_next = jax.lax.all_to_all(known, along_axis, 0, 0)]
    all_to_all x1, waiting for transfers between devices: 20.4 us -> 14.6 us  [copy_for_each(): lax.all_to_all(jnp.broadcast_to(array[None], (peers, *array.shape)), axis...]
    all_gather x1, blocking collectives: 13.4 us -> 17.4 us  [whole_of(): array = lax.all_gather(array, axis, axis=dim, tiled=True)]
    all_gather x1, waiting for transfers between devices: 16.8 us -> 13.8 us  [whole_of(): array = lax.all_gather(array, axis, axis=dim, tiled=True)]
    all_gather x1, waiting for transfers between devices: 36.7 us -> 33.9 us  [collected_together(): both, at, found = (lax.all_gather(jnp.concatenate(lines), axis), 0, {})]
    reshape x0 -> x1, local copies, waits for them, and re-layouts: none -> 2.82 us  [tiles_fit(): newest = jnp.concatenate(e_next, axis=along_dim)]
    all_to_all x1, waiting for transfers between devices: 10.7 us -> 13.4 us  [expert_half(): lax.all_to_all(own_share, EP, split_axis=0, concat_axis=0, tiled=True)]
  transfers between devices with their start and end apart: 6 -> 6, of which waited for: 5 -> 5; matrix products, arithmetic and copies ran while one was open for 13% -> 17% of each run, Pallas kernels for 0% -> 0%
where the time goes in v1:
time: 213 us; the launch traced here: 212 us
  waiting for transfers between devices  76.7 us (36%)
  starting transfers between devices  41.4 us (19%)
  other arithmetic  25.3 us (12%)
  local copies, waits for them, and re-layouts  24.8 us (12%)
  blocking collectives  19.3 us (9%)
  between operations  18.2 us (9%)
  matrix products  6.72 us (3%)
    all_gather x1, waiting for transfers between devices, collected_together(): both, at, found = (lax.all_gather(jnp.concatenate(lines), axis), 0, {})  33.9 us
    all_gather x1, blocking collectives, whole_of(): array = lax.all_gather(array, axis, axis=dim, tiled=True)  17.4 us
    all_to_all x1, starting transfers between devices, expert_half(): lax.all_to_all(own_share, EP, split_axis=0, concat_axis=0, tiled=True)  15.5 us
    all_to_all x1, waiting for transfers between devices, copy_for_each(): lax.all_to_all(jnp.broadcast_to(array[None], (peers, *array.shape)), axis...  14.6 us
    all_gather x1, waiting for transfers between devices, whole_of(): array = lax.all_gather(array, axis, axis=dim, tiled=True)  13.8 us
    all_to_all x1, waiting for transfers between devices, expert_half(): lax.all_to_all(own_share, EP, split_axis=0, concat_axis=0, tiled=True)  13.4 us
    mul x1, other arithmetic, retention_half(): entering = before + jnp.exp(leading)[:, :, None, None] * incoming[1][None]  11.4 us
    all_to_all x1, starting transfers between devices, expert_half(): lax.all_to_all(expert_out, EP, split_axis=0, concat_axis=0, tiled=True)  10.1 us
  transfers between devices with their start and end apart: 6, of which 5 were waited for; matrix products, arithmetic and copies ran while one was open for 17% of the time, Pallas kernels for 0%

profile of v1, /device:TPU:2, one launch (start us, length us, event | category | flops | bytes accessed | tf_op | source)
XLA Modules:
  0.0 212.4 jit_solution(13796839068858657062)
XLA Ops:
  7.2 1.0 copy.45
  8.2 0.1 eq.29
  8.3 0.1 eq.25
  8.4 0.7 broadcast_multiply_fusion
  9.1 1.2 reduce-window.18
  10.3 0.2 slice_reduce_fusion
  10.6 0.1 copy.44
  10.7 0.1 mul.536
  11.0 2.4 %scatter_custom_fusion = s32[512]{0:T(512)S(1)} fusion(s32[512]{0:T(512)S(1)} %bitcast.174, s32[512]{0:T(512)S(1)} %add_select_fusion, s32[]{:T(128)} %constant.60.clone.1), kind=kCustom, calls=%fused_computation.126 | custom fusion | bytes 2052 | tf_op jit(solution)/shard_map/scatter | solution.py:181
  13.5 0.7 convert_element_type.89
  14.2 1.5 fusion
  15.7 0.3 fusion.2
  16.0 3.3 %gather_fusion = bf16[512,2048]{1,0:T(8,128)(2,1)} fusion(bf16[256,2048]{1,0:T(8,128)(2,1)S(1)} %fusion.2, s32[1024]{0:T(1024)S(1)} %pad_clamp_fusion.1), kind=kCustom, calls=%fused_computation | custom fusion | bytes 4196352 | tf_op jit(solution)/shard_map/gather | solution.py:183
  19.4 1.5 constant_dynamic-slice_fusion.1
  20.9 0.5 broadcast.372
  21.4 1.4 reduce.10
  22.8 0.7 reshape.666
  23.5 15.5 %all-to-all-start = ((bf16[32,2,1024]{2,1,0:T(2,128)(2,1)}), bf16[32,2,1024]{2,1,0:T(2,128)(2,1)S(1)}, u32[]{:S(2)}, u32[]{:S(2)}) async-start(bf16[32,2,1024]{2,1,0:T(2,128)(2,1)} %reshape.666), calls=%async_computation | async-start | bytes 262144 | tf_op jit(solution)/shard_map/all_to_all | solution.py:189
  39.0 0.1 copy.41
  39.1 0.2 reduce_window_sum.33
  39.3 0.6 slice_reduce_fusion.1
  40.7 0.6 pad_bitcast_fusion.1
  41.4 1.2 fusion.33
  42.6 0.1 fusion.38
  42.7 13.4 %all-to-all-done = bf16[32,2,1024]{2,1,0:T(2,128)(2,1)S(1)} async-done(((bf16[32,2,1024]{2,1,0:T(2,128)(2,1)}), bf16[32,2,1024]{2,1,0:T(2,128)(2,1)S(1)}, u32[]{:S(2)}, u32[]{:S(2)}) %all-to-all-start) | async-done | bytes 131104 | tf_op jit(solution)/shard_map/all_to_all | solution.py:189
  56.4 1.6 broadcast_in_dim.33
  58.0 7.6 %all-to-all-start.1 = ((bf16[16,32,1,2048]{3,1,2,0:T(8,128)(2,1)}), bf16[16,32,1,2048]{3,1,2,0:T(8,128)(2,1)S(1)}, u32[]{:S(2)}, u32[]{:S(2)}) async-start(bf16[16,32,1,2048]{3,1,2,0:T(8,128)(2,1)} %broadcast_in_dim.33), calls=%async_computation.1 | async-start | bytes 4194304 | tf_op jit(solution)/shard_map/all_to_all | solution.py:74
  65.6 0.6 fusion.79
  66.2 0.4 convolution_bitcast_fusion.1
  66.6 5.2 %while.13 = (s32[]{:T(128)}, f32[1,128,128]{2,1,0:T(8,128)S(1)}, f32[2,1,128,128]{3,2,1,0:T(8,128)}, f32[2,1]{0,1:T(1,128)}, f32[2,1,128,128]{3,2,1,0:T(8,128)S(1)}, /*index=5*/s32[]{:T(128)}, s32[]{:T(128)}) while((s32[]{:T(128)}, f32[1,128,128]{2,1,0:T(8,128)S(1)}, f32[2,1,128,128]{3,2,1,0:T(8,128)}, f32[2,1]{0,1:T(1,128)}, ...), condition=%wide.region_2.3_spmd.clone, body=%wide.region_1.2_spmd.clone.sunk | while | flops 65539 | bytes 328300 | solution.py:140
  66.6 0.6 bitcast_dynamic-update-slice_fusion.2
  67.2 1.3 fusion.87
  68.5 0.6 bitcast_add_fusion.2
  69.2 0.6 bitcast_dynamic-update-slice_fusion.2
  69.8 1.3 fusion.87
  71.1 0.6 bitcast_add_fusion.2
  71.8 1.9 all-gather.2
  73.7 0.5 fusion.78
  76.0 0.6 fusion.65
  76.6 0.6 maximum_bitcast_fusion.1
  77.2 14.6 %all-to-all-done.1 = bf16[16,32,1,2048]{3,1,2,0:T(8,128)(2,1)S(1)} async-done(((bf16[16,32,1,2048]{3,1,2,0:T(8,128)(2,1)}), bf16[16,32,1,2048]{3,1,2,0:T(8,128)(2,1)S(1)}, u32[]{:S(2)}, u32[]{:S(2)}) %all-to-all-start.1) | async-done | bytes 2097184 | tf_op jit(solution)/shard_map/all_to_all | solution.py:74
  91.8 0.7 fusion.5
  92.6 0.5 copy-done.16
  93.0 0.7 fusion.10
  93.8 0.2 copy.49
  93.9 2.4 %stack.2 = bf16[16,32,16,256]{3,2,1,0:T(8,128)(2,1)} broadcast(bf16[32,16,256]{2,1,0:T(8,128)(2,1)S(1)} %copy.49), dimensions={1,2,3} | broadcast | bytes 4456448 | tf_op jit(solution)/shard_map/stack | solution.py:16
  96.3 8.1 %all-to-all-start.2 = ((bf16[16,32,16,256]{3,2,1,0:T(8,128)(2,1)}), bf16[16,32,16,256]{3,2,1,0:T(8,128)(2,1)}, u32[]{:S(2)}, u32[]{:S(2)}) async-start(bf16[16,32,16,256]{3,2,1,0:T(8,128)(2,1)} %stack.2), calls=%async_computation.2 | async-start | bytes 8388608 | tf_op jit(solution)/shard_map/all_to_all | solution.py:17
  104.5 0.2 reduce-window.14
  105.4 33.9 %all-gather.9.cloned.1.call-done = f32[16,129,128]{2,1,0:T(8,128)} async-done(((f32[1,129,128]{2,1,0:T(8,128)}), f32[16,129,128]{2,1,0:T(8,128)}) %all-gather.9.cloned.1.call-update) | async-done | bytes 1056784 | tf_op jit(solution)/shard_map/all_gather | solution.py:36
  139.2 0.8 slice.250
  140.1 0.6 fusion.77
  141.3 11.4 %fusion.56 = f32[128,128]{1,0:T(8,128)S(1)} fusion(f32[16,129,128]{2,1,0:T(8,128)} %all-gather.9.cloned.1.call-done, f32[2,129,128]{2,1,0:T(8,128)S(1)} %all-gather.2, f32[]{:T(128)} %bitcast.46, f32[]{:T(128)} %bitcast.45, f32[]{:T(128)} %bitcast.44, f32[]{:T(128)} %bitcast.43, f32[]{:T(128)} %bitcast.42, f32[]{:T(128)} %bitcast.41, f32[]{:T(128)} %bitcast.40, ...), kind=kLoop, calls=%fused_computation.80 | loop fusion | flops 884736 | bytes 1245278 | tf_op jit(solution)/shard_map/mul | solution.py:146
  152.8 0.3 fusion.14
  153.1 0.4 fusion.39
  153.6 17.4 %all_gather.22 = bf16[256,512]{1,0:T(8,128)(2,1)} all-gather(bf16[256,128]{1,0:T(8,128)(2,1)S(1)} %fusion.49), channel_id=1, replica_groups=mesh['ep_0'=16,'ep_1'=2,'tp_0'=4,'tp_1'=4] {'tp_1'}, dimensions={1}, use_global_device_ids=true | all-gather | bytes 327680 | tf_op jit(solution)/shard_map/all_gather | solution.py:62
  171.1 2.8 %copy.55 = bf16[16,32,2,8,256]{4,3,0,2,1:T(8,128)(2,1)S(1)} copy(bf16[16,32,2,8,256]{4,3,2,1,0:T(8,128)(2,1)} %bitcast.82) | data formatting | bytes 8388608 | tf_op jit(solution)/shard_map/reshape | solution.py:18
  173.9 1.9 convolution_convert_fusion
  175.8 10.1 %all-to-all-start.3 = ((bf16[32,16,128]{2,1,0:T(8,128)(2,1)}), bf16[32,16,128]{2,1,0:T(8,128)(2,1)S(1)}, u32[]{:S(2)}, u32[]{:S(2)}) async-start(bf16[32,16,128]{2,1,0:T(8,128)(2,1)} %convolution_convert_fusion), calls=%async_computation.3 | async-start | bytes 262144 | tf_op jit(solution)/shard_map/all_to_all | solution.py:197
  186.0 0.1 copy.51
  186.1 13.8 %all-gather.7.cloned.1.call-done = bf16[256,2048]{1,0:T(8,128)(2,1)} async-done(((bf16[256,512]{1,0:T(8,128)(2,1)}), bf16[256,2048]{1,0:T(8,128)(2,1)}) %all-gather.7.cloned.1.call-update) | async-done | bytes 1048592 | tf_op jit(solution)/shard_map/all_gather | solution.py:62
  200.0 2.3 %convolution_convert_fusion.1 = bf16[256,128]{1,0:T(8,128)(2,1)} fusion(bf16[256,2048]{1,0:T(8,128)(2,1)} %all-gather.7.cloned.1.call-done, bf16[2048,128]{1,0:T(8,128)(2,1)S(1)} %copy-done.2), kind=kOutput, calls=%fused_computation.24 | convolution fusion | flops 134250496 | bytes 1638400 | tf_op jit(solution)/shard_map/dot_general | solution.py:160
  202.3 0.9 all-to-all-done.3
  203.2 1.3 gather_fusion.1
  204.5 1.1 fusion.19
  (65 shorter events, 0.9 us)
Async XLA Ops:
  7.2 84.7 %copy-start = (bf16[1,2048,256]{2,1,0:T(8,128)(2,1)S(1)}, bf16[1,2048,256]{2,1,0:T(8,128)(2,1)}, u32[]{:S(2)}) copy-start(bf16[1,2048,256]{2,1,0:T(8,128)(2,1)} %param.25) | copy-start | bytes 3145732
  7.2 8.5 %copy-start.1 = (bf16[256,2048]{1,0:T(8,128)(2,1)S(1)}, bf16[256,2048]{1,0:T(8,128)(2,1)}, u32[]{:S(2)}) copy-start(bf16[256,2048]{1,0:T(8,128)(2,1)} %param.21) | copy-start | bytes 3145732
  16.0 23.0 %copy-start.14 = (f32[256,1]{0,1:T(1,128)S(1)}, f32[256,1]{0,1:T(1,128)}, u32[]{:S(2)}) copy-start(f32[256,1]{0,1:T(1,128)} %param.19) | copy-start | bytes 3076
  16.0 24.6 %copy-start.5 = (bf16[256,128]{1,0:T(8,128)(2,1)S(1)}, bf16[256,128]{1,0:T(8,128)(2,1)}, u32[]{:S(2)}) copy-start(bf16[256,128]{1,0:T(8,128)(2,1)} %param.16) | copy-start | bytes 196612
  16.0 24.6 %copy-start.6 = (bf16[256,128]{1,0:T(8,128)(2,1)S(1)}, bf16[256,128]{1,0:T(8,128)(2,1)}, u32[]{:S(2)}) copy-start(bf16[256,128]{1,0:T(8,128)(2,1)} %param.15) | copy-start | bytes 196612
  23.5 32.7 %all-to-all-start = ((bf16[32,2,1024]{2,1,0:T(2,128)(2,1)}), bf16[32,2,1024]{2,1,0:T(2,128)(2,1)S(1)}, u32[]{:S(2)}, u32[]{:S(2)}) async-start(bf16[32,2,1024]{2,1,0:T(2,128)(2,1)} %reshape.666), calls=%async_computation | async-start | bytes 262144 | tf_op jit(solution)/shard_map/all_to_all | solution.py:189
  40.0 25.7 %copy-start.12 = (f32[2]{0:T(128)}, f32[2]{0:T(128)S(1)}, u32[]{:S(2)}) copy-start(f32[2]{0:T(128)S(1)} %get-tuple-element.71) | copy-start | bytes 28
  58.0 8.2 %copy-start.7 = (bf16[256,128]{1,0:T(8,128)(2,1)S(1)}, bf16[256,128]{1,0:T(8,128)(2,1)}, u32[]{:S(2)}) copy-start(bf16[256,128]{1,0:T(8,128)(2,1)} %param.17) | copy-start | bytes 196612
  58.0 13.8 %copy-start.15 = (f32[1,128]{1,0:T(1,128)S(1)}, f32[1,128]{1,0:T(1,128)}, u32[]{:S(2)}) copy-start(f32[1,128]{1,0:T(1,128)} %pad_bitcast_fusion.1) | copy-start | bytes 1540
  58.0 33.8 %all-to-all-start.1 = ((bf16[16,32,1,2048]{3,1,2,0:T(8,128)(2,1)}), bf16[16,32,1,2048]{3,1,2,0:T(8,128)(2,1)S(1)}, u32[]{:S(2)}, u32[]{:S(2)}) async-start(bf16[16,32,1,2048]{3,1,2,0:T(8,128)(2,1)} %broadcast_in_dim.33), calls=%async_computation.1 | async-start | bytes 4194304 | tf_op jit(solution)/shard_map/all_to_all | solution.py:74
  65.6 73.6 %all-gather.9.cloned.1.call-start = ((), (), s32[]{:S(2)}) async-start(), calls=%async_computation.5 | async-start | bytes 1183744 | tf_op jit(solution)/shard_map/all_gather | solution.py:36
  91.8 1.2 copy-start.16
  96.3 8.2 %copy-start.13 = (f32[2,1]{0,1:T(1,128)S(1)}, f32[2,1]{0,1:T(1,128)}, u32[]{:S(2)}) copy-start(f32[2,1]{0,1:T(1,128)} %get-tuple-element.177) | copy-start | bytes 28
  96.3 56.4 %copy-start.3 = (bf16[256,1,64]{2,0,1:T(8,128)(2,1)S(1)}, bf16[256,1,64]{2,0,1:T(8,128)(2,1)}, u32[]{:S(2)}) copy-start(bf16[256,1,64]{2,0,1:T(8,128)(2,1)} %get-tuple-element.83) | copy-start | bytes 98308
  96.3 56.4 %copy-start.4 = (f32[2,1,128,128]{3,2,1,0:T(8,128)S(1)}, f32[2,1,128,128]{3,2,1,0:T(8,128)}, u32[]{:S(2)}) copy-start(f32[2,1,128,128]{3,2,1,0:T(8,128)} %get-tuple-element.30) | copy-start | bytes 393220
  96.3 56.4 %copy-start.10 = (f32[2,128]{1,0:T(2,128)S(1)}, f32[2,128]{1,0:T(2,128)}, u32[]{:S(2)}) copy-start(f32[2,128]{1,0:T(2,128)} %get-tuple-element.106) | copy-start | bytes 3076
  96.3 56.8 %copy-start.8 = (bf16[256,128]{1,0:T(8,128)(2,1)S(1)}, bf16[256,128]{1,0:T(8,128)(2,1)}, u32[]{:S(2)}) copy-start(bf16[256,128]{1,0:T(8,128)(2,1)} %param.17) | copy-start | bytes 196612
  96.3 74.7 %all-to-all-start.2 = ((bf16[16,32,16,256]{3,2,1,0:T(8,128)(2,1)}), bf16[16,32,16,256]{3,2,1,0:T(8,128)(2,1)}, u32[]{:S(2)}, u32[]{:S(2)}) async-start(bf16[16,32,16,256]{3,2,1,0:T(8,128)(2,1)} %stack.2), calls=%async_computation.2 | async-start | bytes 8388608 | tf_op jit(solution)/shard_map/all_to_all | solution.py:17
  104.4 49.1 %copy-start.9 = (bf16[256,128]{1,0:T(8,128)(2,1)S(1)}, bf16[256,128]{1,0:T(8,128)(2,1)}, u32[]{:S(2)}) copy-start(bf16[256,128]{1,0:T(8,128)(2,1)} %param.18) | copy-start | bytes 196612
  104.5 95.5 %all-gather.7.cloned.1.call-start = ((), (), s32[]{:S(2)}) async-start(), calls=%async_computation.4 | async-start | bytes 1310720 | tf_op jit(solution)/shard_map/all_gather | solution.py:62
  171.1 2.8 %copy-start.17 = (bf16[1,4096,128]{2,1,0:T(8,128)(2,1)S(1)}, bf16[1,4096,128]{2,1,0:T(8,128)(2,1)}, u32[]{:S(2)}) copy-start(bf16[1,4096,128]{2,1,0:T(8,128)(2,1)} %param.27) | copy-start | bytes 3145732
  173.9 12.1 %copy-start.11 = (f32[256,2]{0,1:T(2,128)S(1)}, f32[256,2]{0,1:T(2,128)}, u32[]{:S(2)}) copy-start(f32[256,2]{0,1:T(2,128)} %param.24) | copy-start | bytes 6148
  173.9 26.1 %copy-start.2 = (bf16[2048,128]{1,0:T(8,128)(2,1)S(1)}, bf16[2048,128]{1,0:T(8,128)(2,1)}, u32[]{:S(2)}) copy-start(bf16[2048,128]{1,0:T(8,128)(2,1)} %param.20) | copy-start | bytes 1572868
  175.8 27.3 %all-to-all-start.3 = ((bf16[32,16,128]{2,1,0:T(8,128)(2,1)}), bf16[32,16,128]{2,1,0:T(8,128)(2,1)S(1)}, u32[]{:S(2)}, u32[]{:S(2)}) async-start(bf16[32,16,128]{2,1,0:T(8,128)(2,1)} %convolution_convert_fusion), calls=%async_computation.3 | async-start | bytes 262144 | tf_op jit(solution)/shard_map/all_to_all | solution.py:197
Sparse Core Ops, SparseCore 0:
  77.3 61.8 all-gather.8
  171.2 28.7 all-gather.6
